TPU v7x, 128 devices: a whole 4x4x4 slice. The times are simulated.
128 devices in a mesh: rep: 2 (over z_hi), fs: 32 (over z_lo, y, x), tp: 2 (over core).
Axes of the slice: x: 4, y: 4, z: 4 (z_hi: 2, z_lo: 2; z = z_hi * 2 + z_lo), core: 2. Of those that a mesh axis runs over, the one named last changes fastest.
Arguments:
- tokens: bfloat16 [65536, 2048], P(('rep', 'fs', 'tp')), parts along dimension 0, may hold values from -6 to 6
- mix_gain: float32 [2048], replicated, may hold values from 0.1 to 1.9
- w_query: bfloat16 [2048, 512], P('fs', 'tp'), may hold values from -0.125 to 0.125
- w_key: bfloat16 [2048, 512], P('fs', 'tp'), may hold values from -0.125 to 0.125
- w_value: bfloat16 [2048, 1024], P('fs', 'tp'), may hold values from -0.125 to 0.125
- w_out: bfloat16 [1024, 2048], P('tp', 'fs'), may hold values from -0.1875 to 0.1875
- ffn_gain: float32 [2048], replicated, may hold values from 0.1 to 1.9
- w_ffgate: bfloat16 [2048, 2816], P('fs', 'tp'), may hold values from -0.125 to 0.125
- w_ffup: bfloat16 [2048, 2816], P('fs', 'tp'), may hold values from -0.125 to 0.125
- conv_gate: float32 [3, 2816], replicated, may hold values from -3 to 3
- conv_up: float32 [3, 2816], replicated, may hold values from -3 to 3
- w_down: bfloat16 [2816, 2048], P('tp', 'fs'), may hold values from -0.109375 to 0.109375
Outputs:
- layer_out: bfloat16 [65536, 2048], P(('rep', 'fs', 'tp')), parts along dimension 0
There are 2 independent parts, one for each index of `rep`. A program takes and returns all parts, laid end to end along the dimension named above; an argument that names none is the same for every part. Nothing has to cross between parts.
All inputs are finite; a program needn't handle non-finite values.
Results may differ from a plain program's by a relative error of at most 0.014.
Values may be sent and summed in bfloat16 or wider, within the bound.
No kernel may reach another device: no remote copies, remote signals or barrier semaphores. Data moves between devices by JAX's collectives and lax.ppermute only.
A program may use at most 128 MiB of HBM per device.

v0:
```python
import jax
import jax.numpy as jnp
from jax import lax
from jax.sharding import PartitionSpec as P

HEADS = 4
DK = 128
DV = 256
KERNEL = 3
BLOCK = 128
LENGTH = 1024
epsilon = 1e-06


def in_one_piece(arrays, axis, dim, along):
    both = jnp.concatenate(arrays, axis=along)
    out, at, done = (lax.all_gather(both, axis, axis=dim, tiled=True), 0, [])
    for a in arrays:
        done.append(lax.slice_in_dim(out, at, at + a.shape[along], axis=along))
        at += a.shape[along]
    return tuple(done)


def copy_for_each(shard, axis):
    length = lax.axis_size(axis)
    return lax.all_to_all(
        jnp.broadcast_to(shard[None], (length, *shard.shape)), axis, 0, 0, tiled=True
    )


def in_order(pieces, dim):
    pieces = jnp.moveaxis(pieces, 0, dim)
    dims = pieces.shape
    return pieces.reshape(*dims[:dim], dims[dim] * dims[dim + 1], *dims[dim + 2 :])


def collect(shard, axis, dim):
    pieces = copy_for_each(shard, axis)
    return in_order(pieces, dim)


def in_blocks(shard, dim, length):
    dims = shard.shape
    pieces = shard.reshape(*dims[:dim], length, dims[dim] // length, *dims[dim + 1 :])
    return jnp.moveaxis(pieces, dim, 0)


def sent_and_summed(shard, axis, dim):
    length = lax.axis_size(axis)
    pieces = lax.all_to_all(in_blocks(shard, dim, length), axis, 0, 0, tiled=True)
    return jnp.sum(pieces.astype(jnp.float32), axis=0)


def rms_rows(matrix, scale_vec):
    values = matrix.astype(jnp.float32)
    factor = lax.rsqrt(jnp.mean(values * values, axis=-1, keepdims=True) + epsilon)
    return (values * factor * scale_vec).astype(jnp.bfloat16)


def rotate_heads(matrix):
    length = matrix.shape[0]
    half_width = matrix.shape[-1] // 2
    inverse = 10000.0 ** (-jnp.arange(half_width, dtype=jnp.float32) * 2.0 / (2 * half_width))
    angles = jnp.arange(length, dtype=jnp.float32)[:, None] * inverse[None, :]
    cosine = jnp.cos(angles)[:, None, :]
    sine = jnp.sin(angles)[:, None, :]
    values = matrix.astype(jnp.float32)
    first_half = values[..., :half_width]
    second_half = values[..., half_width:]
    return jnp.concatenate(
        [first_half * cosine - second_half * sine, first_half * sine + second_half * cosine],
        axis=-1,
    )


def retain_blocks(rot_query, rot_key, value, rates, block_len):
    length, head_count, width_k = rot_query.shape
    width_v = value.shape[-1]
    blocks = length // block_len
    query4 = rot_query.reshape(blocks, block_len, head_count, width_k)
    key4 = rot_key.reshape(blocks, block_len, head_count, width_k)
    value4 = value.reshape(blocks, block_len, head_count, width_v)
    places = jnp.arange(block_len, dtype=jnp.float32)
    spacing = places[:, None] - places[None, :]
    inside = jnp.where(
        spacing[None] >= 0, jnp.exp(-jnp.maximum(spacing, 0.0)[None] * rates[:, None, None]), 0.0
    )
    scores = jnp.einsum("cihd,cjhd->chij", query4, key4, preferred_element_type=jnp.float32)
    weights = (scores * inside[None]).astype(jnp.bfloat16)
    inner_part = jnp.einsum("chij,cjhe->cihe", weights, value4, preferred_element_type=jnp.float32)
    tail_decay = jnp.exp(-(block_len - 1.0 - places)[:, None] * rates[None, :])
    decayed = (key4.astype(jnp.float32) * tail_decay[None, :, :, None]).astype(jnp.bfloat16)
    states = jnp.einsum("cjhd,cjhe->chde", decayed, value4, preferred_element_type=jnp.float32)
    passing = jnp.exp(-block_len * rates)[:, None, None]

    def advance(carried, fresh):
        return (carried * passing + fresh, carried)

    _, before = lax.scan(advance, jnp.zeros((head_count, width_k, width_v), jnp.float32), states)
    onset_decay = jnp.exp(-(places + 1.0)[:, None] * rates[None, :])
    cross_part = (
        jnp.einsum("cihd,chde->cihe", query4.astype(jnp.float32), before)
        * onset_decay[None, :, :, None]
    )
    return (inner_part + cross_part).reshape(length, head_count, width_v)


def head_norm(retained):
    average = jnp.mean(retained, axis=-1, keepdims=True)
    centered = retained - average
    return centered * lax.rsqrt(jnp.mean(centered * centered, axis=-1, keepdims=True) + epsilon)


def causal_taps(matrix, kernel_w):
    length = matrix.shape[0]
    padded = jnp.pad(matrix.astype(jnp.float32), ((KERNEL - 1, 0), (0, 0)))
    total = jnp.zeros((length, matrix.shape[1]), jnp.float32)
    for tap_idx in range(KERNEL):
        total = total + kernel_w[tap_idx][None, :] * padded[tap_idx : tap_idx + length]
    return total


def collect_ffn(w_ffgate, w_ffup):
    return in_one_piece((w_ffgate, w_ffup), "fs", 0, 1)


def body(
    tokens,
    mix_gain,
    w_query,
    w_key,
    w_value,
    w_out,
    ffn_gain,
    w_ffgate,
    w_ffup,
    conv_gate,
    conv_up,
    w_down,
):
    tp_rank = lax.axis_index("tp")
    heads_here = w_query.shape[1] // DK
    ffn_pair = None
    normed = rms_rows(tokens, mix_gain)
    query_w, key_w, value_w = in_one_piece((w_query, w_key, w_value), "fs", 0, 1)
    qk_cols = query_w.shape[1]
    pieces = lax.all_gather(normed, "tp", axis=0, tiled=True)
    joined = jnp.concatenate(
        [
            jnp.dot(pieces, query_w, preferred_element_type=jnp.float32),
            jnp.dot(pieces, key_w, preferred_element_type=jnp.float32),
            jnp.dot(pieces, value_w, preferred_element_type=jnp.float32),
        ],
        axis=1,
    ).astype(jnp.bfloat16)
    length = joined.shape[0]
    query = joined[:, :qk_cols].reshape(length, heads_here, DK)
    key = joined[:, qk_cols : 2 * qk_cols].reshape(length, heads_here, DK)
    value = joined[:, 2 * qk_cols :].reshape(length, heads_here, DV)
    rot_query = rotate_heads(query).astype(jnp.bfloat16)
    rot_key = (rotate_heads(key) * DK ** (-0.5)).astype(jnp.bfloat16)
    head_ids = (tp_rank * heads_here + jnp.arange(heads_here, dtype=jnp.int32)).astype(jnp.float32)
    rates = 1.0 / 16.0 * (32.0 / LENGTH) ** (head_ids / (HEADS - 1))
    retained = retain_blocks(rot_query, rot_key, value, rates, BLOCK)
    hidden = head_norm(retained).reshape(length, heads_here * DV).astype(jnp.bfloat16)
    out_full = collect(w_out, "fs", 1)
    mix_sum = sent_and_summed(
        jnp.dot(hidden, out_full, preferred_element_type=jnp.float32).astype(jnp.bfloat16), "tp", 0
    )
    resid = (tokens.astype(jnp.float32) + mix_sum).astype(jnp.bfloat16)
    normed_ffn = rms_rows(resid, ffn_gain)
    ff_here = w_ffgate.shape[1]
    ffn_pair = collect_ffn(w_ffgate, w_ffup)
    gate_w, up_w = ffn_pair
    pieces = lax.all_gather(normed_ffn, "tp", axis=0, tiled=True)
    both_pre = jnp.concatenate(
        [
            jnp.dot(pieces, gate_w, preferred_element_type=jnp.float32),
            jnp.dot(pieces, up_w, preferred_element_type=jnp.float32),
        ],
        axis=1,
    ).astype(jnp.bfloat16)
    gate_pre = both_pre[:, :ff_here]
    up_pre = both_pre[:, ff_here:]
    gate_taps = lax.dynamic_slice_in_dim(conv_gate, tp_rank * ff_here, ff_here, 1)
    up_taps = lax.dynamic_slice_in_dim(conv_up, tp_rank * ff_here, ff_here, 1)
    activ = (jax.nn.silu(causal_taps(gate_pre, gate_taps)) * causal_taps(up_pre, up_taps)).astype(
        jnp.bfloat16
    )
    down_full = lax.all_gather(w_down, "fs", axis=1, tiled=True)
    ffn_sum = sent_and_summed(
        jnp.dot(activ, down_full, preferred_element_type=jnp.float32).astype(jnp.bfloat16), "tp", 0
    )
    return (resid.astype(jnp.float32) + ffn_sum).astype(jnp.bfloat16)


def solution(mesh):
    placed = (
        P(("rep", "fs", "tp"), None),
        P(),
        P("fs", "tp"),
        P("fs", "tp"),
        P("fs", "tp"),
        P("tp", "fs"),
        P(),
        P("fs", "tp"),
        P("fs", "tp"),
        P(),
        P(),
        P("tp", "fs"),
    )
    return jax.shard_map(
        body, mesh=mesh, in_specs=placed, out_specs=P(("rep", "fs", "tp"), None), check_vma=False
    )
```

profile of v0, /device:TPU:1, one launch (start us, length us, event | category | flops | bytes accessed | tf_op | source)
XLA Modules:
  0.0 637.9 jit_solution(8390424234193751009)
XLA Ops:
  6.6 2.1 fusion.6
  8.7 3.5 fusion.8
  13.0 1.5 broadcast_in_dim.25
  14.5 9.3 %all-to-all-start = ((bf16[32,512,64]{1,2,0:T(8,128)(2,1)}), bf16[32,512,64]{1,2,0:T(8,128)(2,1)}, u32[]{:S(2)}, u32[]{:S(2)}) async-start(bf16[32,512,64]{1,2,0:T(8,128)(2,1)} %broadcast_in_dim.25), calls=%async_computation | async-start | bytes 4194304 | tf_op jit(solution)/shard_map/all_to_all | solution.py:26
  24.2 1.0 fusion.44
  25.2 7.1 %all-gather.6.cloned.1.call-done = bf16[1024,2048]{1,0:T(8,128)(2,1)} async-done(((bf16[512,2048]{1,0:T(8,128)(2,1)}), bf16[1024,2048]{1,0:T(8,128)(2,1)}) %all-gather.6.cloned.1.call-update) | async-done | bytes 4194320 | tf_op jit(solution)/shard_map/all_gather | solution.py:147
  32.3 140.7 %all-gather.8.cloned.1.call-done = bf16[2048,1024]{1,0:T(8,128)(2,1)} async-done(((bf16[64,1024]{1,0:T(8,128)(2,1)}), bf16[2048,1024]{1,0:T(8,128)(2,1)}) %all-gather.8.cloned.1.call-update) | async-done | bytes 4194320 | tf_op jit(solution)/shard_map/all_gather | solution.py:17
  173.0 3.9 convolution_convert_fusion.3
  177.1 2.5 convolution_convert_fusion.2
  179.7 1.1 subtract_convert_fusion
  181.8 6.2 fusion.31
  187.9 1.3 reshape_reshape.3
  191.0 6.5 %while.13 = (s32[]{:T(128)}, f32[2,128,256]{2,1,0:T(8,128)S(1)}, bf16[8,2,128,256]{3,2,1,0:T(8,128)(2,1)}, f32[8,2,128,256]{3,2,1,0:T(8,128)S(1)}, s32[]{:T(128)}, /*index=5*/s32[]{:T(128)}, s32[]{:T(128)}) while((s32[]{:T(128)}, f32[2,128,256]{2,1,0:T(8,128)S(1)}, bf16[8,2,128,256]{3,2,1,0:T(8,128)(2,1)}, ...), condition=%wide.region_2.3_spmd.clone, body=%wide.region_1.2_spmd.clone.sunk | while | flops 262155 | bytes 1180272 | solution.py:99
  197.5 1.0 copy.48
  198.8 1.2 copy.49
  200.3 3.2 fusion.45
  203.6 3.0 fusion.54
  207.5 0.9 fusion.29
  208.9 4.0 convolution_convert_fusion.1
  212.9 27.5 %all_to_all.15 = bf16[2,512,2048]{2,1,0:T(8,128)(2,1)S(1)} all-to-all(bf16[2,512,2048]{2,1,0:T(8,128)(2,1)S(1)} %bitcast.73), channel_id=1, replica_groups=mesh['rep'=2,'fs'=32,'tp'=2] {'tp'}, dimensions={0} | all-to-all | bytes 8388608 | tf_op jit(solution)/shard_map/all_to_all | solution.py:50
  240.4 1.0 convert_reduce_fusion.1
  242.7 1.9 fusion.12
  246.0 1.1 dynamic-slice_reduce_fusion.2
  247.1 15.1 %all-gather.10.cloned.1.call-done = bf16[1024,2048]{1,0:T(8,128)(2,1)} async-done(((bf16[512,2048]{1,0:T(8,128)(2,1)}), bf16[1024,2048]{1,0:T(8,128)(2,1)}) %all-gather.10.cloned.1.call-update) | async-done | bytes 4194320 | tf_op jit(solution)/shard_map/all_gather | solution.py:175
  262.2 155.1 %all-gather.12.cloned.1.call-done = bf16[2048,2816]{1,0:T(8,128)(2,1)} async-done(((bf16[64,2816]{1,0:T(8,128)(2,1)}), bf16[2048,2816]{1,0:T(8,128)(2,1)}) %all-gather.12.cloned.1.call-update) | async-done | bytes 11534352 | tf_op jit(solution)/shard_map/all_gather | solution.py:17
  417.3 11.8 %fusion.17 = f32[1024,1408]{1,0:T(8,128)} fusion(bf16[1024,2048]{1,0:T(8,128)(2,1)} %all-gather.10.cloned.1.call-done, bf16[2048,2816]{1,0:T(8,128)(2,1)} %all-gather.12.cloned.1.call-done), kind=kOutput, calls=%fused_computation.26 | convolution fusion | flops 5908463616 | bytes 15728640 | tf_op jit(solution)/shard_map/dot_general | solution.py:178
  429.1 8.5 %fusion.23 = f32[1024,1408]{1,0:T(8,128)} fusion(bf16[1024,2048]{1,0:T(8,128)(2,1)S(1)} %copy-done.13, bf16[2048,2816]{1,0:T(8,128)(2,1)S(1)} %copy-done.11), kind=kOutput, calls=%fused_computation.28 | convolution fusion | flops 5908463616 | bytes 15728640 | tf_op jit(solution)/shard_map/dot_general | solution.py:179
  437.6 139.5 %all-gather.14.cloned.1.call-done = bf16[1408,2048]{0,1:T(8,128)(2,1)} async-done(((bf16[1408,64]{0,1:T(8,128)(2,1)}), bf16[1408,2048]{0,1:T(8,128)(2,1)}) %all-gather.14.cloned.1.call-update) | async-done | bytes 5767184 | tf_op jit(solution)/shard_map/all_gather | solution.py:190
  577.1 23.0 %convolution_convert_fusion = bf16[1024,2048]{1,0:T(8,128)(2,1)} fusion(bf16[1408,2048]{0,1:T(8,128)(2,1)} %all-gather.14.cloned.1.call-done, f32[1024,1408]{1,0:T(8,128)} %fusion.23, f32[1024,1408]{1,0:T(8,128)} %fusion.17, f32[1408]{0:T(1024)S(1)} %get-tuple-element.59, f32[1408]{0:T(1024)S(1)} %get-tuple-element.58, f32[1408]{0:T(1024)S(1)} %get-tuple-element.57, ...), kind=kOutput, calls=%fused_computation.29 | convolution fusion | flops 5930745856 | bytes 21529600 | tf_op jit(solution)/shard_map/dot_general | solution.py:192
  600.1 28.2 %all_to_all.16 = bf16[2,512,2048]{2,1,0:T(8,128)(2,1)S(1)} all-to-all(bf16[2,512,2048]{2,1,0:T(8,128)(2,1)} %bitcast.72), channel_id=1, replica_groups=mesh['rep'=2,'fs'=32,'tp'=2] {'tp'}, dimensions={0} | all-to-all | bytes 8388608 | tf_op jit(solution)/shard_map/all_to_all | solution.py:50
  628.3 1.0 convert_reduce_fusion
  629.3 2.1 fusion.13
  (92 shorter events, 15.0 us)
Async XLA Ops:
  6.5 5.7 copy-start.7
  6.5 5.7 copy-start.8
  6.5 5.7 copy-start.9
  6.5 6.4 %copy-start.6 = (bf16[512,64]{0,1:T(8,128)(2,1)S(1)}, bf16[512,64]{0,1:T(8,128)(2,1)}, u32[]{:S(2)}) copy-start(bf16[512,64]{0,1:T(8,128)(2,1)} %param.19) | copy-start | bytes 196612
  6.5 25.8 %all-gather.6.cloned.1.call-start = ((), (), s32[]{:S(2)}) async-start(), calls=%async_computation.3 | async-start | bytes 6291456 | tf_op jit(solution)/shard_map/all_gather | solution.py:147
  12.2 160.8 %all-gather.8.cloned.1.call-start = ((), (), s32[]{:S(2)}) async-start(), calls=%async_computation.4 | async-start | bytes 4325376 | tf_op jit(solution)/shard_map/all_gather | solution.py:17
  14.5 194.4 %all-to-all-start = ((bf16[32,512,64]{1,2,0:T(8,128)(2,1)}), bf16[32,512,64]{1,2,0:T(8,128)(2,1)}, u32[]{:S(2)}, u32[]{:S(2)}) async-start(bf16[32,512,64]{1,2,0:T(8,128)(2,1)} %broadcast_in_dim.25), calls=%async_computation | async-start | bytes 4194304 | tf_op jit(solution)/shard_map/all_to_all | solution.py:26
  23.9 238.3 %all-gather.10.cloned.1.call-start = ((), (), s32[]{:S(2)}) async-start(), calls=%async_computation.5 | async-start | bytes 6291456 | tf_op jit(solution)/shard_map/all_gather | solution.py:175
  173.0 4.1 copy-start.12
  189.6 0.8 copy-start.1
  198.8 4.8 copy-start.2
  200.3 3.2 copy-start.3
  240.4 1.6 copy-start
  241.9 0.7 copy-start.10
  242.6 2.0 copy-start.4
  242.6 2.0 copy-start.5
  244.6 172.7 %all-gather.12.cloned.1.call-start = ((), (), s32[]{:S(2)}) async-start(), calls=%async_computation.6 | async-start | bytes 11894784 | tf_op jit(solution)/shard_map/all_gather | solution.py:17
  245.4 331.7 %all-gather.14.cloned.1.call-start = ((), (), s32[]{:S(2)}) async-start(), calls=%async_computation.7 | async-start | bytes 5947392 | tf_op jit(solution)/shard_map/all_gather | solution.py:190
  417.3 11.8 %copy-start.11 = (bf16[2048,2816]{1,0:T(8,128)(2,1)S(1)}, bf16[2048,2816]{1,0:T(8,128)(2,1)}, u32[]{:S(2)}) copy-start(bf16[2048,2816]{1,0:T(8,128)(2,1)} %all-gather.12.cloned.1.call-done) | copy-start | bytes 34603012
  417.3 11.9 %copy-start.13 = (bf16[1024,2048]{1,0:T(8,128)(2,1)S(1)}, bf16[1024,2048]{1,0:T(8,128)(2,1)}, u32[]{:S(2)}) copy-start(bf16[1024,2048]{1,0:T(8,128)(2,1)} %all-gather.10.cloned.1.call-done) | copy-start | bytes 12582916
Sparse Core Ops, SparseCore 0:
  12.3 19.9 all-gather.5
  34.0 138.9 all-gather.7
  244.7 17.4 all-gather.9
  263.7 153.5 all-gather.11
  418.8 158.2 all-gather.13
where the time goes:
time: 639 us; the launch traced here: 638 us
  waiting for transfers between devices  458 us (72%)
  matrix products  66.7 us (10%)
  blocking collectives  55.7 us (9%)
  other arithmetic  24.3 us (4%)
  between operations  13.5 us (2%)
  local copies, waits for them, and re-layouts  9.83 us (2%)
  starting transfers between devices  9.54 us (1%)
    all_gather x2, waiting for transfers between devices, in_one_piece(): out, at, done = (lax.all_gather(both, axis, axis=dim, tiled=True), 0, [])  296 us
    all_gather x1, waiting for transfers between devices, body(): down_full = lax.all_gather(w_down, 'fs', axis=1, tiled=True)  139 us
    all_to_all x2, blocking collectives, sent_and_summed(): lax.all_to_all(in_blocks(shard, dim, length), axis, 0, 0, tiled=True)  55.7 us
    dot_general x1, matrix products, body(): jnp.dot(activ, down_full, preferred_element_type=jnp.float32)  23 us
    all_gather x1, waiting for transfers between devices, body(): pieces = lax.all_gather(normed_ffn, 'tp', axis=0, tiled=True)  15.1 us
  transfers between devices with their start and end apart: 6, of which 5 were waited for; matrix products, arithmetic and copies ran while one was open for 9% of the time, Pallas kernels for 0%

commit v1 on v0

--- a/solution.py
+++ b/solution.py
@@ -10,6 +10,13 @@
 BLOCK = 128
 LENGTH = 1024
 epsilon = 1e-06
+
+
+def swapped_in(value, mesh_axis, along):
+    size = lax.axis_size(mesh_axis)
+    shards = jnp.stack([value for _ in range(size)])
+    shards = lax.all_to_all(shards, mesh_axis, split_axis=0, concat_axis=0)
+    return jnp.concatenate(shards, axis=along)
 
 
 def in_one_piece(arrays, axis, dim, along):
@@ -187,7 +194,7 @@
     activ = (jax.nn.silu(causal_taps(gate_pre, gate_taps)) * causal_taps(up_pre, up_taps)).astype(
         jnp.bfloat16
     )
-    down_full = lax.all_gather(w_down, "fs", axis=1, tiled=True)
+    down_full = swapped_in(w_down, "fs", 1)
     ffn_sum = sent_and_summed(
         jnp.dot(activ, down_full, preferred_element_type=jnp.float32).astype(jnp.bfloat16), "tp", 0
     )

time: 639 us -> 544 us (0.85)
  waiting for transfers between devices: 458 us -> 356 us
  starting transfers between devices: 9.54 us -> 16.1 us
    all_gather x1 -> x0, waiting for transfers between devices: 139 us -> none  [body(): down_full = lax.all_gather(w_down, 'fs', axis=1, tiled=True)]
    all_gather x2, waiting for transfers between devices: 296 us -> 343 us  [in_one_piece(): out, at, done = (lax.all_gather(both, axis, axis=dim, tiled=True), 0, [])]
    all_gather x1, waiting for transfers between devices: 15.1 us -> 6.05 us  [body(): pieces = lax.all_gather(normed_ffn, 'tp', axis=0, tiled=True)]
    all_to_all x0 -> x1, starting transfers between devices: none -> 6.61 us  [swapped_in(): shards = lax.all_to_all(shards, mesh_axis, split_axis=0, concat_axis=0)]
  transfers between devices with their start and end apart: 6 -> 6, of which waited for: 5 -> 4; matrix products, arithmetic and copies ran while one was open for 9% -> 12% of each run, Pallas kernels for 0% -> 0%
where the time goes in v1:
time: 544 us; the launch traced here: 542 us
  waiting for transfers between devices  356 us (65%)
  matrix products  67.1 us (12%)
  blocking collectives  51.8 us (10%)
  other arithmetic  25.1 us (5%)
  starting transfers between devices  16.1 us (3%)
  between operations  13.5 us (2%)
  local copies, waits for them, and re-layouts  12.2 us (2%)
    all_gather x2, waiting for transfers between devices, in_one_piece(): out, at, done = (lax.all_gather(both, axis, axis=dim, tiled=True), 0, [])  343 us
    all_to_all x2, blocking collectives, sent_and_summed(): lax.all_to_all(in_blocks(shard, dim, length), axis, 0, 0, tiled=True)  51.8 us
    dot_general x1, matrix products, body(): jnp.dot(activ, down_full, preferred_element_type=jnp.float32)  22.4 us
    dot_general x1, matrix products, body(): jnp.dot(pieces, gate_w, preferred_element_type=jnp.float32)  11.8 us
  transfers between devices with their start and end apart: 6, of which 4 were waited for; matrix products, arithmetic and copies ran while one was open for 12% of the time, Pallas kernels for 0%

profile of v1, /device:TPU:1, one launch (start us, length us, event | category | flops | bytes accessed | tf_op | source)
XLA Modules:
  0.0 542.2 jit_solution(1547383030648804760)
XLA Ops:
  6.6 2.1 fusion.6
  8.7 3.5 fusion.8
  13.0 1.5 broadcast_in_dim.25
  14.5 9.3 %all-to-all-start = ((bf16[32,512,64]{1,2,0:T(8,128)(2,1)}), bf16[32,512,64]{1,2,0:T(8,128)(2,1)}, u32[]{:S(2)}, u32[]{:S(2)}) async-start(bf16[32,512,64]{1,2,0:T(8,128)(2,1)} %broadcast_in_dim.25), calls=%async_computation | async-start | bytes 4194304 | tf_op jit(solution)/shard_map/all_to_all | solution.py:33
  24.2 1.0 fusion.44
  25.2 7.1 %all-gather.5.cloned.1.call-done = bf16[1024,2048]{1,0:T(8,128)(2,1)} async-done(((bf16[512,2048]{1,0:T(8,128)(2,1)}), bf16[1024,2048]{1,0:T(8,128)(2,1)}) %all-gather.5.cloned.1.call-update) | async-done | bytes 4194320 | tf_op jit(solution)/shard_map/all_gather | solution.py:154
  32.3 140.6 %all-gather.7.cloned.1.call-done = bf16[2048,1024]{1,0:T(8,128)(2,1)} async-done(((bf16[64,1024]{1,0:T(8,128)(2,1)}), bf16[2048,1024]{1,0:T(8,128)(2,1)}) %all-gather.7.cloned.1.call-update) | async-done | bytes 4194320 | tf_op jit(solution)/shard_map/all_gather | solution.py:24
  172.9 3.9 convolution_convert_fusion.3
  177.0 2.5 convolution_convert_fusion.2
  179.6 1.1 subtract_convert_fusion
  181.7 6.2 %fusion.31 = bf16[1024,512]{1,0:T(8,128)(2,1)} fusion(bf16[1024,2048]{1,0:T(8,128)(2,1)} %all-gather.5.cloned.1.call-done, bf16[2048,1024]{1,0:T(8,128)(2,1)} %all-gather.7.cloned.1.call-done), kind=kOutput, calls=%fused_computation.39 | convolution fusion | flops 2148007936 | bytes 7340032 | tf_op jit(solution)/shard_map/dot_general | solution.py:159
  187.8 1.3 reshape_reshape.3
  189.2 1.1 fusion.37
  190.3 1.6 fusion.38
  191.9 6.5 %while.13 = (s32[]{:T(128)}, f32[2,128,256]{2,1,0:T(8,128)S(1)}, bf16[8,2,128,256]{3,2,1,0:T(8,128)(2,1)}, f32[8,2,128,256]{3,2,1,0:T(8,128)S(1)}, s32[]{:T(128)}, /*index=5*/s32[]{:T(128)}, s32[]{:T(128)}) while((s32[]{:T(128)}, f32[2,128,256]{2,1,0:T(8,128)S(1)}, bf16[8,2,128,256]{3,2,1,0:T(8,128)(2,1)}, ...), condition=%wide.region_2.3_spmd.clone, body=%wide.region_1.2_spmd.clone.sunk | while | flops 262155 | bytes 1180272 | solution.py:106
  198.4 1.0 copy.49
  199.7 1.2 copy.50
  201.2 3.2 fusion.45
  204.5 3.0 fusion.54
  209.8 4.0 convolution_convert_fusion.1
  213.8 27.3 %all_to_all.20 = bf16[2,512,2048]{2,1,0:T(8,128)(2,1)S(1)} all-to-all(bf16[2,512,2048]{2,1,0:T(8,128)(2,1)S(1)} %bitcast.76), channel_id=1, replica_groups=mesh['rep'=2,'fs'=32,'tp'=2] {'tp'}, dimensions={0} | all-to-all | bytes 8388608 | tf_op jit(solution)/shard_map/all_to_all | solution.py:57
  243.4 1.9 fusion.12
  246.2 3.2 stack.2
  249.4 6.6 %all-to-all-start.2 = ((bf16[32,1408,64]{1,2,0:T(8,128)(2,1)}), bf16[32,1408,64]{1,2,0:T(8,128)(2,1)}, u32[]{:S(2)}, u32[]{:S(2)}) async-start(bf16[32,1408,64]{1,2,0:T(8,128)(2,1)} %stack.2), calls=%async_computation.2 | async-start | bytes 11534336 | tf_op jit(solution)/shard_map/all_to_all | solution.py:18
  256.0 1.0 dynamic-slice_reduce_fusion.2
  257.0 6.0 %all-gather.9.cloned.1.call-done = bf16[1024,2048]{1,0:T(8,128)(2,1)} async-done(((bf16[512,2048]{1,0:T(8,128)(2,1)}), bf16[1024,2048]{1,0:T(8,128)(2,1)}) %all-gather.9.cloned.1.call-update) | async-done | bytes 4194320 | tf_op jit(solution)/shard_map/all_gather | solution.py:182
  263.1 202.3 %all-gather.11.cloned.1.call-done = bf16[2048,2816]{1,0:T(8,128)(2,1)} async-done(((bf16[64,2816]{1,0:T(8,128)(2,1)}), bf16[2048,2816]{1,0:T(8,128)(2,1)}) %all-gather.11.cloned.1.call-update) | async-done | bytes 11534352 | tf_op jit(solution)/shard_map/all_gather | solution.py:24
  465.4 11.8 %fusion.17 = f32[1024,1408]{1,0:T(8,128)} fusion(bf16[1024,2048]{1,0:T(8,128)(2,1)} %all-gather.9.cloned.1.call-done, bf16[2048,2816]{1,0:T(8,128)(2,1)} %all-gather.11.cloned.1.call-done), kind=kOutput, calls=%fused_computation.26 | convolution fusion | flops 5908463616 | bytes 15728640 | tf_op jit(solution)/shard_map/dot_general | solution.py:185
  477.2 8.5 %fusion.23 = f32[1024,1408]{1,0:T(8,128)} fusion(bf16[1024,2048]{1,0:T(8,128)(2,1)S(1)} %copy-done.13, bf16[2048,2816]{1,0:T(8,128)(2,1)S(1)} %copy-done.11), kind=kOutput, calls=%fused_computation.28 | convolution fusion | flops 5908463616 | bytes 15728640 | tf_op jit(solution)/shard_map/dot_general | solution.py:186
  485.7 22.4 %convolution_convert_fusion = bf16[1024,2048]{1,0:T(8,128)(2,1)} fusion(bf16[1408,2048]{0,1:T(8,128)(2,1)} %bitcast.14, f32[1024,1408]{1,0:T(8,128)} %fusion.23, f32[1024,1408]{1,0:T(8,128)} %fusion.17, f32[1408]{0:T(1024)S(1)} %get-tuple-element.59, f32[1408]{0:T(1024)S(1)} %get-tuple-element.58, f32[1408]{0:T(1024)S(1)} %get-tuple-element.57, ...), kind=kOutput, calls=%fused_computation.29 | convolution fusion | flops 5930745856 | bytes 21529600 | tf_op jit(solution)/shard_map/dot_general | solution.py:199
  508.1 24.5 %all_to_all.21 = bf16[2,512,2048]{2,1,0:T(8,128)(2,1)S(1)} all-to-all(bf16[2,512,2048]{2,1,0:T(8,128)(2,1)} %bitcast.75), channel_id=1, replica_groups=mesh['rep'=2,'fs'=32,'tp'=2] {'tp'}, dimensions={0} | all-to-all | bytes 8388608 | tf_op jit(solution)/shard_map/all_to_all | solution.py:57
  533.6 2.1 fusion.13
  (92 shorter events, 15.5 us)
Async XLA Ops:
  6.5 5.7 %copy-start.9 = (bf16[64,256]{1,0:T(8,128)(2,1)S(1)}, bf16[64,256]{1,0:T(8,128)(2,1)}, u32[]{:S(2)}) copy-start(bf16[64,256]{1,0:T(8,128)(2,1)} %param.16) | copy-start | bytes 98308
  6.5 5.7 %copy-start.8 = (bf16[64,256]{1,0:T(8,128)(2,1)S(1)}, bf16[64,256]{1,0:T(8,128)(2,1)}, u32[]{:S(2)}) copy-start(bf16[64,256]{1,0:T(8,128)(2,1)} %param.17) | copy-start | bytes 98308
  6.5 5.7 %copy-start.7 = (bf16[64,512]{1,0:T(8,128)(2,1)S(1)}, bf16[64,512]{1,0:T(8,128)(2,1)}, u32[]{:S(2)}) copy-start(bf16[64,512]{1,0:T(8,128)(2,1)} %param.18) | copy-start | bytes 196612
  6.5 6.4 %copy-start.6 = (bf16[512,64]{0,1:T(8,128)(2,1)S(1)}, bf16[512,64]{0,1:T(8,128)(2,1)}, u32[]{:S(2)}) copy-start(bf16[512,64]{0,1:T(8,128)(2,1)} %param.19) | copy-start | bytes 196612
  6.5 25.8 %all-gather.5.cloned.1.call-start = ((), (), s32[]{:S(2)}) async-start(), calls=%async_computation.4 | async-start | bytes 6291456 | tf_op jit(solution)/shard_map/all_gather | solution.py:154
  12.2 160.7 %all-gather.7.cloned.1.call-start = ((), (), s32[]{:S(2)}) async-start(), calls=%async_computation.5 | async-start | bytes 4325376 | tf_op jit(solution)/shard_map/all_gather | solution.py:24
  14.5 195.2 %all-to-all-start = ((bf16[32,512,64]{1,2,0:T(8,128)(2,1)}), bf16[32,512,64]{1,2,0:T(8,128)(2,1)}, u32[]{:S(2)}, u32[]{:S(2)}) async-start(bf16[32,512,64]{1,2,0:T(8,128)(2,1)} %broadcast_in_dim.25), calls=%async_computation | async-start | bytes 4194304 | tf_op jit(solution)/shard_map/all_to_all | solution.py:33
  23.9 239.2 %all-gather.9.cloned.1.call-start = ((), (), s32[]{:S(2)}) async-start(), calls=%async_computation.6 | async-start | bytes 6291456 | tf_op jit(solution)/shard_map/all_gather | solution.py:182
  172.9 4.1 copy-start.12
  199.7 4.8 copy-start.1
  201.2 3.2 copy-start.2
  241.1 1.6 copy-start
  242.7 0.7 copy-start.10
  243.4 2.0 copy-start.4
  243.4 2.0 copy-start.5
  243.4 2.8 copy-start.3
  245.3 220.1 %all-gather.11.cloned.1.call-start = ((), (), s32[]{:S(2)}) async-start(), calls=%async_computation.7 | async-start | bytes 11894784 | tf_op jit(solution)/shard_map/all_gather | solution.py:24
  249.4 236.3 %all-to-all-start.2 = ((bf16[32,1408,64]{1,2,0:T(8,128)(2,1)}), bf16[32,1408,64]{1,2,0:T(8,128)(2,1)}, u32[]{:S(2)}, u32[]{:S(2)}) async-start(bf16[32,1408,64]{1,2,0:T(8,128)(2,1)} %stack.2), calls=%async_computation.2 | async-start | bytes 11534336 | tf_op jit(solution)/shard_map/all_to_all | solution.py:18
  465.4 11.8 %copy-start.11 = (bf16[2048,2816]{1,0:T(8,128)(2,1)S(1)}, bf16[2048,2816]{1,0:T(8,128)(2,1)}, u32[]{:S(2)}) copy-start(bf16[2048,2816]{1,0:T(8,128)(2,1)} %all-gather.11.cloned.1.call-done) | copy-start | bytes 34603012
  465.4 11.8 %copy-start.13 = (bf16[1024,2048]{1,0:T(8,128)(2,1)S(1)}, bf16[1024,2048]{1,0:T(8,128)(2,1)}, u32[]{:S(2)}) copy-start(bf16[1024,2048]{1,0:T(8,128)(2,1)} %all-gather.9.cloned.1.call-done) | copy-start | bytes 12582916
Sparse Core Ops, SparseCore 0:
  12.3 19.9 all-gather.4
  34.0 138.8 all-gather.6
  245.4 17.5 all-gather.8
  264.6 200.8 all-gather.10
